TPU v7x, 32 devices: a whole 2x2x4 slice. The times are simulated.
32 devices in a mesh: gr: 2 (over x), fs: 8 (over z, y), tp: 2 (over core).
Axes of the slice: x: 2, y: 2, z: 4, core: 2. Of those that a mesh axis runs over, the one named last changes fastest.
Arguments:
- tokens: bfloat16 [4096, 2048], P(('gr', 'tp'), 'fs'), may hold values from -400 to 400
- norm_gain: float32 [2048], P('fs'), may hold values from 0.1 to 1.9
- up_weight: float32 [2048, 8192], P('fs', ('gr', 'tp')), may hold values from -0.125 to 0.125
- down_weight: float32 [8192, 2048], P('fs', ('gr', 'tp')), may hold values from -0.09375 to 0.09375
Outputs:
- mixed: bfloat16 [2048, 4096], P('fs', ('gr', 'tp'))
- up_ready: bfloat16 [2048, 8192], P(None, 'fs')
- down_ready: bfloat16 [8192, 2048], P('fs')
All inputs are finite; a program needn't handle non-finite values.
Results may differ from a plain program's by a relative error of at most 0.023.
Values may be sent and summed in bfloat16 or wider, within the bound.
A program may use at most 64 MiB of HBM per device.

v0:
```python
import functools

import jax
import jax.numpy as jnp
from jax import lax
from jax.experimental import pallas as pl
from jax.experimental.pallas import tpu as pltpu
from jax.sharding import PartitionSpec as P

MESH = pl.DeviceIdType.MESH
epsilon = 1e-06


def line_shape(count):
    short = max(d for d in range(1, count + 1) if count % d == 0 and d * d <= count)
    return count // short, short


def chunks(total, size):
    return min(total, size)


def kernel(
    G, n, T, Z, Y, k, E,
    tok_ref, gain_ref, upw_ref, dnw_ref,
    mixed_ref, up_full, dn_full,
    up_bf, xbuf, tok_full, hidden, part, ybuf, zup, zdn,
    tok_recv, tok_su, tok_sd, tok_sy,
    x_recv, x_send, up_recv, up_s, up_sx, up_st,
    dn_recv, dn_sx, dn_st,
    y_recv, y_send, zu_recv, zu_send, zd_recv, zd_send,
):
    g, f, t = lax.axis_index("gr"), lax.axis_index("fs"), lax.axis_index("tp")
    z, y = f // Y, f % Y
    q = g * T + t
    rows = upw_ref.shape[0]
    sub = rows // G
    unit = up_full.shape[1]
    dcols = dnw_ref.shape[1]
    pending = []

    def send(src, dst, ssem, rsem, dev, cond=None):
        copy = pltpu.make_async_remote_copy(
            src_ref=src, dst_ref=dst, send_sem=ssem, recv_sem=rsem, device_id=dev, device_id_type=MESH
        )
        if cond is None:
            copy.start()
        else:
            pl.when(cond)(copy.start)
        pending.append((cond, copy))

    def arrived(ref, sem):
        pltpu.make_async_copy(ref, ref, sem).wait()

    slab = tok_ref.shape[0] // E

    def owns(e):
        return pltpu.make_async_copy(tok_ref.at[pl.ds(e * slab, slab)], tok(f, e), tok_recv.at[f, e])

    def tok(c, e):
        return tok_full.at[c, pl.ds(e * slab, slab)]

    for e in range(E):
        owns(e).start()

    def pass_tokens(zc, e, src, up, down):
        c = zc * Y + y
        dst = tok(c, e)
        if up is not None:
            send(src, dst, tok_su.at[zc, e], tok_recv.at[c, e], (g, f + Y, t), up)
        if down is not None:
            send(src, dst, tok_sd.at[zc, e], tok_recv.at[c, e], (g, f - Y, t), down)

    def cross_tokens(zc, e, src, cond):
        c = zc * Y + y
        for o in range(1, Y):
            y2 = (y + o) % Y
            send(src, tok(c, e), tok_sy.at[zc, o, e], tok_recv.at[c, e], (g, z * Y + y2, t), cond)

    for e in range(E):
        mine = tok_ref.at[pl.ds(e * slab, slab)]
        pass_tokens(z, e, mine, z < Z - 1, z > 0)
        cross_tokens(z, e, mine, None)

    step = chunks(rows, 32)
    for j in range(k):
        @pl.loop(0, rows // step)
        def _(i):
            r = pl.ds(pl.multiple_of(i * step, step), step)
            up_bf[j, r, :] = (gain_ref[r, :] * upw_ref[r, pl.ds(j * unit, unit)]).astype(jnp.bfloat16)

    def piece(c, h):
        return up_full.at[pl.ds(pl.multiple_of(c * rows + h * sub, sub), sub)]

    def to_owner(j, slot, source_q, src):
        owner = source_q * k + j
        local = pltpu.make_async_copy(src, piece(f, g), up_recv.at[f, g])
        pl.when(owner == f)(local.start)
        send(src, piece(f, g), up_s.at[j, slot], up_recv.at[f, g], (g, owner, t), owner != f)

    def half(j, h):
        return up_bf.at[j, pl.ds(pl.multiple_of(h * sub, sub), sub)]

    for oh in range(1, G):
        h = (g + oh) % G
        for j in range(k):
            send(half(j, h), xbuf.at[G - oh, j], x_send.at[j, oh], x_recv.at[j, G - oh], (h, f, t))
    for j in range(k):
        to_owner(j, 0, q, half(j, g))

    def dn_block(index):
        return dn_full.at[:, pl.ds(pl.multiple_of(index * dcols, dcols), dcols)]

    deep = dnw_ref.shape[0]
    dstep = chunks(deep, 64)

    @pl.loop(0, deep // dstep)
    def _(i):
        r = pl.ds(pl.multiple_of(i * dstep, dstep), dstep)
        dn_full[r, pl.ds(pl.multiple_of(q * dcols, dcols), dcols)] = dnw_ref[r, :].astype(jnp.bfloat16)

    for o in range(1, G):
        send(dn_block(q), dn_block(q), dn_sx.at[o], dn_recv.at[q], ((g + o) % G, f, t))
    for o in range(1, T):
        send(dn_block(q), dn_block(q), dn_st.at[0, o], dn_recv.at[q], (g, f, (t + o) % T))

    star = (f // k) % T
    is_star = t == star

    def relay_direct(c, cond):
        ok = is_star & cond

        @pl.when(ok)
        def _():
            arrived(piece(c, g), up_recv.at[c, g])
        for o in range(1, G):
            send(piece(c, g), piece(c, g), up_sx.at[c, o], up_recv.at[c, g], ((g + o) % G, f, t), ok)
        for o in range(1, T):
            send(piece(c, g), piece(c, g), up_st.at[c, 0, o], up_recv.at[c, g], (g, f, (t + o) % T), ok)

    def relay_far(c, cond):
        ok = is_star & cond
        for oh in range(1, G):
            h = (g + oh) % G

            @pl.when(ok)
            def _():
                arrived(piece(c, h), up_recv.at[c, h])
            for o in range(1, T):
                send(piece(c, h), piece(c, h), up_st.at[c, oh, o], up_recv.at[c, h], (g, f, (t + o) % T), ok)

    for og in range(1, G):
        for j in range(k):
            arrived(xbuf.at[og, j], x_recv.at[j, og])
            to_owner(j, og, ((g + og) % G) * T + t, xbuf.at[og, j])
    for e in range(E):
        owns(e).wait()

    earlier = []
    for s in range(Z):
        now = []
        if s == 0:
            now = [(z * Y + (y + o) % Y, True) for o in range(Y)]
        else:
            lower, upper = z - s >= 0, z + s < Z
            zl, zu = jnp.maximum(z - s, 0), jnp.minimum(z + s, Z - 1)

            for e in range(E):
                @pl.when(lower)
                def _():
                    arrived(tok(zl * Y + y, e), tok_recv.at[zl * Y + y, e])
                pass_tokens(zl, e, tok(zl * Y + y, e), lower & (z < Z - 1), None)
                cross_tokens(zl, e, tok(zl * Y + y, e), lower)

                @pl.when(upper)
                def _():
                    arrived(tok(zu * Y + y, e), tok_recv.at[zu * Y + y, e])
                pass_tokens(zu, e, tok(zu * Y + y, e), None, upper & (z > 0))
                cross_tokens(zu, e, tok(zu * Y + y, e), upper)
            for o in range(Y):
                now.append((zl * Y + (y + o) % Y, lower))
                now.append((zu * Y + (y + o) % Y, upper))
        for c, cond in now:
            relay_direct(c, cond)
        for c, cond in earlier:
            relay_far(c, cond)
        earlier = now
        if s == 1 % Z:
            for o in range(1, G):
                index = ((g + o) % G) * T + t
                arrived(dn_block(index), dn_recv.at[index])
                for ot in range(1, T):
                    send(dn_block(index), dn_block(index), dn_st.at[o, ot], dn_recv.at[index], (g, f, (t + ot) % T))
    for c, cond in earlier:
        relay_far(c, cond)

    for zc in range(Z):
        for o in range(1, Y):
            c = zc * Y + (y + o) % Y
            for e in range(E):
                arrived(tok(c, e), tok_recv.at[c, e])

    @pl.when(jnp.logical_not(is_star))
    def _():
        @pl.loop(0, n)
        def _(c):
            for h in range(G):
                arrived(piece(c, h), up_recv.at[c, h])

    tokens_here = tok_ref.shape[0]
    tile = chunks(tokens_here, 256)
    width = n * tok_ref.shape[1]

    @pl.loop(0, tokens_here // tile)
    def _(i):
        r = pl.ds(pl.multiple_of(i * tile, tile), tile)
        blocks = [tok_full[c, r, :] for c in range(n)]
        squares = None
        for block in blocks:
            wide = block.astype(jnp.float32)
            total = jnp.sum(wide * wide, axis=1, keepdims=True)
            squares = total if squares is None else squares + total
        scale = lax.rsqrt(squares / width + epsilon)
        raw = jnp.dot(jnp.concatenate(blocks, axis=1), up_full[...], preferred_element_type=jnp.float32)
        hidden[r, :] = jnp.square(jnp.maximum(raw * scale, 0.0)).astype(jnp.bfloat16)

    for o in range(G):
        for ot in range(1, T):
            index = ((g + o) % G) * T + (t + ot) % T
            arrived(dn_block(index), dn_recv.at[index])

    feat = part.shape[1]

    def nth(o):
        value = jnp.int32(0)
        for zv in range(Z):
            order = sorted(range(Z), key=lambda zd: (-abs(zd - zv), zd))
            value = jnp.where(z == zv, order[o], value)
        return value

    if feat % 128 == 0:
        def compute(c):
            cols = dn_full[:, pl.ds(pl.multiple_of(c * feat, feat), feat)]
            part[c] = lax.dot_general(
                cols.T, hidden[...], (((1,), (1,)), ((), ())), preferred_element_type=jnp.float32
            ).astype(jnp.bfloat16)
    else:
        per = 128 // feat

        @pl.loop(0, n // per)
        def _(b):
            cols = dn_full[:, pl.ds(pl.multiple_of(b * 128, 128), 128)]
            whole = lax.dot_general(
                cols.T, hidden[...], (((1,), (1,)), ((), ())), preferred_element_type=jnp.float32
            ).astype(jnp.bfloat16)
            for p in range(per):
                part[b * per + p] = whole[p * feat:(p + 1) * feat]

        def compute(c):
            pass

    @pl.loop(0, Z)
    def _(i):
        zd = nth_dynamic(i, z, Z)
        for o in range(1, Y):
            y2 = (y + o) % Y
            c = zd * Y + y2
            compute(c)
            pltpu.make_async_remote_copy(
                src_ref=part.at[c], dst_ref=ybuf.at[zd, Y - o], send_sem=y_send.at[zd, o],
                recv_sem=y_recv.at[zd, Y - o], device_id=(g, z * Y + y2, t), device_id_type=MESH,
            ).start()
        compute(zd * Y + y)

    for zd in range(Z):
        for o in range(1, Y):
            c = zd * Y + (y + o) % Y
            pending.append((None, pltpu.make_async_remote_copy(
                src_ref=part.at[c], dst_ref=ybuf.at[zd, Y - o], send_sem=y_send.at[zd, o],
                recv_sem=y_recv.at[zd, Y - o], device_id=(g, z * Y + (y + o) % Y, t), device_id_type=MESH,
            )))

    rstep = chunks(feat, 32)

    def add_up(zd, extras, target, start=None):
        c = zd * Y + y

        @pl.loop(0, feat // rstep)
        def _(i):
            r = pl.ds(pl.multiple_of(i * rstep, rstep), rstep)
            total = part[c, r, :].astype(jnp.float32)
            for o in range(1, Y):
                total = total + ybuf[zd, o, r, :].astype(jnp.float32)
            for extra in extras:
                total = total + extra[zd, r, :].astype(jnp.float32)
            if target is None:
                part[c, r, :] = total.astype(jnp.bfloat16)
            else:
                target[r, :] = total.astype(jnp.bfloat16)

    for i in range(Z):
        zd = nth(i)
        for o in range(1, Y):
            arrived(ybuf.at[zd, o], y_recv.at[zd, o])
        c = zd * Y + y
        going_up, going_down = zd > z, zd < z

        @pl.when(going_up & (z > 0))
        def _():
            arrived(zup.at[zd], zu_recv.at[zd])
            add_up(zd, [zup], None)

        @pl.when(going_up & (z == 0))
        def _():
            add_up(zd, [], None)

        @pl.when(going_down & (z < Z - 1))
        def _():
            arrived(zdn.at[zd], zd_recv.at[zd])
            add_up(zd, [zdn], None)

        @pl.when(going_down & (z == Z - 1))
        def _():
            add_up(zd, [], None)

        send(part.at[c], zup.at[zd], zu_send.at[zd], zu_recv.at[zd], (g, f + Y, t), going_up)
        send(part.at[c], zdn.at[zd], zd_send.at[zd], zd_recv.at[zd], (g, f - Y, t), going_down)

        @pl.when(zd == z)
        def _():
            @pl.when(z > 0)
            def _():
                arrived(zup.at[zd], zu_recv.at[zd])

            @pl.when(z < Z - 1)
            def _():
                arrived(zdn.at[zd], zd_recv.at[zd])

            @pl.when(z == 0)
            def _():
                add_up(zd, [zdn] if Z > 1 else [], mixed_ref)

            if Z > 1:
                @pl.when(z == Z - 1)
                def _():
                    add_up(zd, [zup], mixed_ref)

                @pl.when((z > 0) & (z < Z - 1))
                def _():
                    add_up(zd, [zup, zdn], mixed_ref)

    for cond, copy in pending:
        if cond is None:
            copy.wait_send()
        else:
            pl.when(cond)(copy.wait_send)


def nth_dynamic(i, z, Z):
    value = jnp.int32(0)
    for zv in range(Z):
        order = sorted(range(Z), key=lambda zd: (-abs(zd - zv), zd))
        for o in range(Z):
            value = jnp.where((z == zv) & (i == o), order[o], value)
    return value


def shards(dims, tokens, norm_gain, up_weight, down_weight):
    G, n, T = dims
    Z, Y = line_shape(n)
    rows, cols = up_weight.shape
    here, w = tokens.shape
    deep, dcols = down_weight.shape
    unit = cols * G * T // n
    k = n // (G * T)
    E = 2 if here % 64 == 0 else 1
    width = rows * n
    feat = dcols * G * T // n
    bf = jnp.bfloat16
    dma = pltpu.SemaphoreType.DMA
    vmem = pl.BlockSpec(memory_space=pltpu.VMEM)
    hbm = pl.BlockSpec(memory_space=pl.ANY)
    return pl.pallas_call(
        functools.partial(kernel, G, n, T, Z, Y, k, E),
        out_shape=(
            pltpu.VMEM((feat, here), bf),
            pltpu.VMEM((width, unit), bf),
            pltpu.VMEM((deep, dcols * G * T), bf),
        ),
        in_specs=[vmem] * 4,
        out_specs=(vmem, vmem, vmem),
        scratch_shapes=[
            pltpu.VMEM((k, rows, unit), bf),
            pltpu.VMEM((G, k, rows // G, unit), bf),
            pltpu.VMEM((n, here, w), bf),
            pltpu.VMEM((here, unit), bf),
            pltpu.VMEM((n, feat, here), bf),
            pltpu.VMEM((Z, Y, feat, here), bf),
            pltpu.VMEM((Z, feat, here), bf),
            pltpu.VMEM((Z, feat, here), bf),
            dma((n, E)), dma((Z, E)), dma((Z, E)), dma((Z, Y, E)),
            dma((k, G)), dma((k, G)), dma((n, G)), dma((k, G)), dma((n, G)), dma((n, G, T)),
            dma((G * T,)), dma((G,)), dma((G, T)),
            dma((Z, Y)), dma((Z, Y)), dma((Z,)), dma((Z,)), dma((Z,)), dma((Z,)),
        ],
        compiler_params=pltpu.CompilerParams(has_side_effects=True, vmem_limit_bytes=46 * 1024 * 1024),
    )(tokens, norm_gain[:, None], up_weight, down_weight)


def solution(mesh):
    dims = (mesh.shape["gr"], mesh.shape["fs"], mesh.shape["tp"])
    in_specs = (P(("gr", "tp"), "fs"), P("fs"), P("fs", ("gr", "tp")), P("fs", ("gr", "tp")))
    out_specs = (P("fs", ("gr", "tp")), P(None, "fs"), P("fs", None))
    return jax.shard_map(
        functools.partial(shards, dims), mesh=mesh, in_specs=in_specs, out_specs=out_specs, check_vma=False
    )
```

profile of v0, /device:TPU:0, one launch (start us, length us, event | category | flops | bytes accessed | tf_op | source)
XLA Modules:
  0.0 140.6 jit_solution(10537890352739598059)
XLA Ops:
  0.6 1.5 %copy.7.gain_ref = f32[256,1]{1,0:T(8,128)} copy(f32[256,1]{0,1:T(1,128)} %bitcast.1) | data formatting | bytes 2048 | tf_op jit(solution)/shard_map/broadcast_in_dim | solution.py:407
  2.1 133.7 %shard_map.67 = (bf16[256,1024]{1,0:T(8,128)(2,1)S(1)}, bf16[2048,1024]{1,0:T(8,128)(2,1)S(1)}, bf16[1024,2048]{1,0:T(8,128)(2,1)S(1)}) custom-call(bf16[1024,256]{1,0:T(8,128)(2,1)} %tok_ref.1, f32[256,1]{1,0:T(8,128)} %copy.7.gain_ref, f32[256,2048]{1,0:T(8,128)} %upw_ref.1, f32[1024,512]{1,0:T(8,128)} %dnw_ref.1), custom_call_target="tpu_custom_call" | custom-call | tf_op jit(solution)/shard_map/pallas_call | solution.py:383
  135.8 0.8 copy.11
  136.6 2.0 %copy.12 = bf16[2048,1024]{1,0:T(8,128)(2,1)} copy(bf16[2048,1024]{1,0:T(8,128)(2,1)S(1)} %get-tuple-element.4) | data formatting | bytes 8388608
  138.6 2.0 %copy.13 = bf16[1024,2048]{1,0:T(8,128)(2,1)} copy(bf16[1024,2048]{1,0:T(8,128)(2,1)S(1)} %get-tuple-element.5) | data formatting | bytes 8388608
where the time goes:
time: 141 us
  Pallas kernels  134 us (95%)
  local copies, waits for them, and re-layouts  6.29 us (4%)
    pallas_call x1, Pallas kernels, shards(): pl.pallas_call(functools.partial(kernel, G, n, T, Z, Y, k, E), out_shape=...  134 us
    unnamed x3, local copies, waits for them, and re-layouts  4.82 us

commit v1 on v0

v1 whole, which is shorter than its diff:
```python
import functools

import jax
import jax.numpy as jnp
from jax import lax
from jax.experimental import pallas as pl
from jax.experimental.pallas import tpu as pltpu
from jax.sharding import PartitionSpec as P

MESH = pl.DeviceIdType.MESH
epsilon = 1e-06


def line_shape(count):
    short = max(d for d in range(1, count + 1) if count % d == 0 and d * d <= count)
    return count // short, short


def chunks(total, size):
    return min(total, size)


def kernel(
    G, n, T, Z, Y, k, E, early, late, send_count,
    tok_ref, gain_ref, upw_ref, dnw_ref,
    mixed_ref, up_full, dn_full,
    upw_v, dnw_v, gain_v, gain_col, up_bf, xbuf, tok_full, hidden, part,
    ybuf, zup, zdn, zup_late, zdn_late, yfin,
    load_sem, hand, send_sem, tok_recv, x_recv, up_recv, dn_recv,
    y_recv, zu_recv, zd_recv, zul_recv, zdl_recv, yf_recv,
    y_send, zu_send, zd_send, zul_send, zdl_send,
):
    g, f, t = lax.axis_index("gr"), lax.axis_index("fs"), lax.axis_index("tp")
    z, y = f // Y, f % Y
    q = g * T + t
    rows = upw_v.shape[0]
    sub = rows // G
    unit = up_full.shape[1]
    dcols = dnw_v.shape[1]
    feat = part.shape[2]
    here = tok_full.shape[1]
    slab = here // E
    pending = []

    def fresh():
        assert len(pending) < send_count
        return send_sem.at[len(pending)]

    def send(src, dst, rsem, dev, cond=None):
        copy = pltpu.make_async_remote_copy(
            src_ref=src, dst_ref=dst, send_sem=fresh(), recv_sem=rsem, device_id=dev, device_id_type=MESH
        )
        if cond is None:
            copy.start()
        else:
            pl.when(cond)(copy.start)
        pending.append((cond, copy))

    def arrived(ref, sem, cond=None):
        wait = pltpu.make_async_copy(ref, ref, sem).wait
        if cond is None:
            wait()
        else:
            pl.when(cond)(wait)

    def tok(c, e):
        return tok_full.at[c, pl.ds(e * slab, slab)]

    loads = []
    for e in range(E):
        loads.append(pltpu.make_async_copy(tok_ref.at[pl.ds(e * slab, slab)], tok(f, e), tok_recv.at[f, e]))
    loads.append(pltpu.make_async_copy(gain_ref, gain_v, load_sem.at[0]))
    for h in range(G):
        r = pl.ds(h * sub, sub)
        loads.append(pltpu.make_async_copy(upw_ref.at[r], upw_v.at[r], load_sem.at[1 + h]))
    loads.append(pltpu.make_async_copy(dnw_ref, dnw_v, load_sem.at[1 + G]))

    barrier = pltpu.get_barrier_semaphore()
    below, above = z > 0, z < Z - 1
    line = below.astype(jnp.int32) + above.astype(jnp.int32)

    def greet(sem, wide):
        def tell(dev):
            pl.semaphore_signal(sem, inc=1, device_id=dev, device_id_type=MESH)

        pl.when(above)(lambda: tell((g, f + Y, t)))
        pl.when(below)(lambda: tell((g, f - Y, t)))
        for o in range(1, Y):
            tell((g, z * Y + (y + o) % Y, t))
        if wide:
            for o in range(1, G):
                tell(((g + o) % G, f, t))
            for o in range(1, T):
                tell((g, f, (t + o) % T))

    greet(barrier, True)
    for copy in loads:
        copy.start()
    pl.semaphore_wait(barrier, line + (Y - 1) + (G - 1) + (T - 1))

    rounds = Z - 1
    greeted = [0]

    def next_round():
        if greeted[0] < rounds:
            greet(hand.at[greeted[0]], False)
            greeted[0] += 1

    def round_over(i):
        if i < rounds:
            pl.semaphore_wait(hand.at[i], line + (Y - 1))

    next_round()

    for copy in loads[E:E + 1]:
        copy.wait()
    wide_gain = jnp.broadcast_to(gain_v[...], (128, rows))
    gain_col[...] = wide_gain.T

    step = chunks(sub, 32)

    def convert_up(h):
        @pl.loop(0, sub // step)
        def _(i):
            r = pl.ds(pl.multiple_of(h * sub + i * step, step), step)
            column = gain_col[r, 0:1]
            for j in range(k):
                up_bf[j, r, :] = (column * upw_v[r, pl.ds(j * unit, unit)]).astype(jnp.bfloat16)

    def piece(c, h):
        return up_full.at[pl.ds(pl.multiple_of(c * rows + h * sub, sub), sub)]

    def half(j, h):
        return up_bf.at[j, pl.ds(pl.multiple_of(h * sub, sub), sub)]

    def share_tokens(e):
        loads[e].wait()
        own = tok(f, e)
        for o in range(1, Y):
            send(own, own, tok_recv.at[f, e], (g, z * Y + (y + o) % Y, t))
        send(own, own, tok_recv.at[f, e], (g, f + Y, t), above)
        send(own, own, tok_recv.at[f, e], (g, f - Y, t), below)

    share_tokens(0)
    for h in range(G):
        loads[E + 1 + h].wait()
    for oh in range(1, G):
        h = (g + oh) % G
        convert_up(h)
        for j in range(k):
            send(half(j, h), xbuf.at[G - oh, j], x_recv.at[j, G - oh], (h, f, t))
    round_over(0)
    next_round()
    convert_up(g)
    for e in range(1, E):
        share_tokens(e)

    def to_owner(j, source_q, src):
        owner = source_q * k + j
        local = pltpu.make_async_copy(src, piece(f, g), up_recv.at[f, g])
        pl.when(owner == f)(local.start)
        send(src, piece(f, g), up_recv.at[f, g], (g, owner, t), owner != f)

    for i in range(1, rounds):
        round_over(i)
        next_round()
    for j in range(k):
        to_owner(j, q, half(j, g))

    star = (f // k) % T
    is_star = t == star

    def dn_block(index):
        return dn_full.at[:, pl.ds(pl.multiple_of(index * dcols, dcols), dcols)]

    deep = dnw_v.shape[0]
    dstep = chunks(deep, 64)
    loads[E + 1 + G].wait()

    @pl.loop(0, deep // dstep)
    def _(i):
        r = pl.ds(pl.multiple_of(i * dstep, dstep), dstep)
        dn_full[r, pl.ds(pl.multiple_of(q * dcols, dcols), dcols)] = dnw_v[r, :].astype(jnp.bfloat16)

    def down_across(cond):
        for o in range(1, G):
            send(dn_block(q), dn_block(q), dn_recv.at[q], ((g + o) % G, f, t), cond)

    for o in range(1, T):
        send(dn_block(q), dn_block(q), dn_recv.at[q], (g, f, (t + o) % T))

    def relay_direct(c, cond):
        ok = is_star & cond
        arrived(piece(c, g), up_recv.at[c, g], ok)
        for o in range(1, G):
            send(piece(c, g), piece(c, g), up_recv.at[c, g], ((g + o) % G, f, t), ok)
        for o in range(1, T):
            send(piece(c, g), piece(c, g), up_recv.at[c, g], (g, f, (t + o) % T), ok)

    def relay_far(c, cond):
        ok = is_star & cond
        for oh in range(1, G):
            h = (g + oh) % G
            arrived(piece(c, h), up_recv.at[c, h], ok)
            for o in range(1, T):
                send(piece(c, h), piece(c, h), up_recv.at[c, h], (g, f, (t + o) % T), ok)

    def on_tokens(c, e, cond, up, down, cross):
        arrived(tok(c, e), tok_recv.at[c, e], cond)
        if up is not None:
            send(tok(c, e), tok(c, e), tok_recv.at[c, e], (g, f + Y, t), up)
        if down is not None:
            send(tok(c, e), tok(c, e), tok_recv.at[c, e], (g, f - Y, t), down)
        if cross:
            for o in range(1, Y):
                send(tok(c, e), tok(c, e), tok_recv.at[c, e], (g, z * Y + (y + o) % Y, t), cond)

    def from_exchange():
        for og in range(1, G):
            for j in range(k):
                arrived(xbuf.at[og, j], x_recv.at[j, og])
                to_owner(j, ((g + og) % G) * T + t, xbuf.at[og, j])

    for e in early:
        for o in range(1, Y):
            on_tokens(z * Y + (y + o) % Y, e, None, above, below, False)

    def pieces_at(s):
        if s == 0:
            return [(z * Y + (y + o) % Y, True) for o in range(Y)]
        lower, upper = z - s >= 0, z + s < Z
        zl, zu = jnp.maximum(z - s, 0), jnp.minimum(z + s, Z - 1)
        found = []
        for o in range(Y):
            found.append((zl * Y + (y + o) % Y, lower))
            found.append((zu * Y + (y + o) % Y, upper))
        return found

    def tokens_at(s):
        lower, upper = z - s >= 0, z + s < Z
        zl, zu = jnp.maximum(z - s, 0), jnp.minimum(z + s, Z - 1)
        for e in range(E):
            if e in early:
                for o in range(Y):
                    y2 = (y + o) % Y
                    on_tokens(zl * Y + y2, e, lower, lower & above, None, False)
                    on_tokens(zu * Y + y2, e, upper, None, upper & below, False)
            else:
                on_tokens(zl * Y + y, e, lower, lower & above, None, True)
                on_tokens(zu * Y + y, e, upper, None, upper & below, True)

    earlier = []
    for s in range(1, Z + 1):
        if s < Z:
            tokens_at(s)
        if s == 1:
            from_exchange()
            down_across(jnp.logical_not(is_star))
        now = pieces_at(s - 1)
        for c, cond in now:
            relay_direct(c, cond)
        for c, cond in earlier:
            relay_far(c, cond)
        earlier = now
    down_across(is_star)
    for c, cond in earlier:
        relay_far(c, cond)

    @pl.when(jnp.logical_not(is_star))
    def _():
        @pl.loop(0, n)
        def _(c):
            for h in range(G):
                arrived(piece(c, h), up_recv.at[c, h])

    width = n * tok_full.shape[2]

    def span(e):
        return pl.ds(e * slab, slab)

    def layer1(e):
        r = span(e)
        if e not in early:
            for zc in range(Z):
                for o in range(1, Y):
                    c = zc * Y + (y + o) % Y
                    arrived(tok(c, e), tok_recv.at[c, e])
        blocks = [tok_full[c, r, :] for c in range(n)]
        squares = None
        for block in blocks:
            wide = block.astype(jnp.float32)
            total = jnp.sum(wide * wide, axis=1, keepdims=True)
            squares = total if squares is None else squares + total
        scale = lax.rsqrt(squares / width + epsilon)
        raw = jnp.dot(jnp.concatenate(blocks, axis=1), up_full[...], preferred_element_type=jnp.float32)
        hidden[r, :] = jnp.square(jnp.maximum(raw * scale, 0.0)).astype(jnp.bfloat16)

    groups = G if Z % G == 0 else 1
    per_group = Z // groups

    def order(gv, zv, group):
        first = ((gv + group) % groups) * per_group
        return sorted(range(first, first + per_group), key=lambda zd: (-abs(zd - zv), zd))

    def nth(group, i):
        value = jnp.int32(0)
        for gv in range(G):
            for zv in range(Z):
                picks = order(gv, zv, group)
                for o in range(per_group):
                    value = jnp.where((g == gv) & (z == zv) & (i == o), picks[o], value)
        return value

    def cross_copy(zd, o, e):
        y2 = (y + o) % Y
        return pltpu.make_async_remote_copy(
            src_ref=part.at[zd * Y + y2, span(e)], dst_ref=ybuf.at[zd, Y - o, span(e)], send_sem=y_send.at[zd, o, e],
            recv_sem=y_recv.at[zd, Y - o, e], device_id=(g, z * Y + y2, t), device_id_type=MESH,
        )

    def line_copy(zd, e, up):
        c = zd * Y + y
        if up:
            return pltpu.make_async_remote_copy(
                src_ref=part.at[c, span(e)], dst_ref=zup.at[zd, span(e)], send_sem=zu_send.at[zd, e],
                recv_sem=zu_recv.at[zd, e], device_id=(g, f + Y, t), device_id_type=MESH,
            )
        return pltpu.make_async_remote_copy(
            src_ref=part.at[c, span(e)], dst_ref=zdn.at[zd, span(e)], send_sem=zd_send.at[zd, e],
            recv_sem=zd_recv.at[zd, e], device_id=(g, f - Y, t), device_id_type=MESH,
        )

    def late_copy(zd, y2, e, up):
        at = late.index(e)
        here_in = pl.ds(at * slab, slab)
        if up:
            return pltpu.make_async_remote_copy(
                src_ref=part.at[zd * Y + y2, span(e)], dst_ref=zup_late.at[zd, y2, here_in],
                send_sem=zul_send.at[zd, y2, at], recv_sem=zul_recv.at[zd, y2, at],
                device_id=(g, f + Y, t), device_id_type=MESH,
            )
        return pltpu.make_async_remote_copy(
            src_ref=part.at[zd * Y + y2, span(e)], dst_ref=zdn_late.at[zd, y2, here_in],
            send_sem=zdl_send.at[zd, y2, at], recv_sem=zdl_recv.at[zd, y2, at],
            device_id=(g, f - Y, t), device_id_type=MESH,
        )

    def layer2(group, e):
        r = span(e)

        @pl.loop(0, per_group)
        def _(i):
            zd = nth(group, i)
            cols = dn_full[:, pl.ds(pl.multiple_of(zd * (Y * feat), Y * feat), Y * feat)]
            whole = jnp.dot(hidden[r, :], cols, preferred_element_type=jnp.float32).astype(jnp.bfloat16)
            for y2 in range(Y):
                part[zd * Y + y2, r, :] = whole[:, y2 * feat:(y2 + 1) * feat]
            if e not in late:
                for o in range(1, Y):
                    cross_copy(zd, o, e).start()

    rstep = chunks(slab, 32)
    fstep = chunks(slab, 128)

    def add_up(c, e, extras, final=False):
        size = fstep if final else rstep

        @pl.loop(0, slab // size)
        def _(i):
            r = pl.ds(pl.multiple_of(e * slab + i * size, size), size)
            total = part[c, r, :].astype(jnp.float32)
            for ref, base in extras:
                total = total + ref[pl.ds(pl.multiple_of(base + i * size, size), size), :].astype(jnp.float32)
            if final:
                mixed_ref[:, r] = total.T.astype(jnp.bfloat16)
            else:
                part[c, r, :] = total.astype(jnp.bfloat16)

    ends = [
        (jnp.bool_(True), False, False) if Z == 1 else (z == 0, False, True),
    ]
    if Z > 1:
        ends.append((z == Z - 1, True, False))
    if Z > 2:
        ends.append((below & above, True, True))

    def finish(e, low, high, crossed):
        for cond, has_low, has_high in ends:
            extras = list(crossed) + ([low] if has_low else []) + ([high] if has_high else [])

            @pl.when(cond)
            def _():
                add_up(z * Y + y, e, extras, True)

    def reduce_slab(group, e):
        @pl.loop(0, per_group)
        def _(i):
            zd = nth(group, i)
            c = zd * Y + y
            base = e * slab
            crossed = [(ybuf.at[zd, o], base) for o in range(1, Y)]
            low, high = (zup.at[zd], base), (zdn.at[zd], base)
            for o in range(1, Y):
                arrived(ybuf.at[zd, o, span(e)], y_recv.at[zd, o, e])
            arrived(zup.at[zd, span(e)], zu_recv.at[zd, e], (zd >= z) & below)
            arrived(zdn.at[zd, span(e)], zd_recv.at[zd, e], (zd <= z) & above)
            if crossed:
                pl.when(((zd > z) & (z == 0)) | ((zd < z) & (z == Z - 1)))(lambda: add_up(c, e, crossed))
            pl.when((zd > z) & below)(lambda: add_up(c, e, crossed + [low]))
            pl.when((zd < z) & above)(lambda: add_up(c, e, crossed + [high]))
            pl.when(zd > z)(lambda: line_copy(zd, e, True).start())
            pl.when(zd < z)(lambda: line_copy(zd, e, False).start())
            pl.when(zd == z)(lambda: finish(e, low, high, crossed))

    def final_cross(o, e):
        at = late.index(e)
        y2 = (y + o) % Y
        return pltpu.make_async_remote_copy(
            src_ref=part.at[z * Y + y2, span(e)], dst_ref=yfin.at[Y - o, pl.ds(at * slab, slab)],
            send_sem=yf_recv.at[1, o, at], recv_sem=yf_recv.at[0, Y - o, at],
            device_id=(g, z * Y + y2, t), device_id_type=MESH,
        )

    def reduce_late(group, e):
        at = late.index(e)
        base = at * slab
        inside = pl.ds(base, slab)

        @pl.loop(0, per_group)
        def _(i):
            zd = nth(group, i)
            for o in range(1, Y + 1):
                y2 = (y + o) % Y
                c = zd * Y + y2
                low, high = (zup_late.at[zd, y2], base), (zdn_late.at[zd, y2], base)
                arrived(zup_late.at[zd, y2, inside], zul_recv.at[zd, y2, at], (zd >= z) & below)
                arrived(zdn_late.at[zd, y2, inside], zdl_recv.at[zd, y2, at], (zd <= z) & above)
                own = zd == z if o < Y else jnp.bool_(False)
                pl.when((zd > z) & below)(lambda: add_up(c, e, [low]))
                pl.when((zd < z) & above)(lambda: add_up(c, e, [high]))
                if o < Y:
                    for cond, has_low, has_high in ends:
                        extras = ([low] if has_low else []) + ([high] if has_high else [])
                        if extras:
                            pl.when(own & cond)(lambda: add_up(c, e, extras))
                    pl.when(own)(lambda: final_cross(o, e).start())
                pl.when(zd > z)(lambda: late_copy(zd, y2, e, True).start())
                pl.when(zd < z)(lambda: late_copy(zd, y2, e, False).start())

    def finish_late(e):
        at = late.index(e)
        base = at * slab
        for o in range(1, Y):
            arrived(yfin.at[o, pl.ds(base, slab)], yf_recv.at[0, o, at])
        finish(e, (zup_late.at[z, y], base), (zdn_late.at[z, y], base), [(yfin.at[o], base) for o in range(1, Y)])

    slabs = list(late) + [e for e in range(E) if e not in late]

    def reduce_any(group, e):
        if e in late:
            reduce_late(group, e)
        else:
            reduce_slab(group, e)

    waiting = []
    for group in range(groups):
        gd = (g + group) % G
        if groups == 1:
            others = [((g + o) % G) * T + t for o in range(1, G)]
            mine = [((g + o) % G) * T + (t + ot) % T for o in range(G) for ot in range(1, T)]
        elif group == 0:
            others, mine = [], [g * T + (t + ot) % T for ot in range(1, T)]
        else:
            others, mine = [gd * T + t], [gd * T + (t + ot) % T for ot in range(1, T)]
        for index in others:
            arrived(dn_block(index), dn_recv.at[index])
            for ot in range(1, T):
                send(dn_block(index), dn_block(index), dn_recv.at[index], (g, f, (t + ot) % T))
        for count, e in enumerate(slabs):
            if group == 0:
                layer1(e)
            if count == 0:
                for index in mine:
                    arrived(dn_block(index), dn_recv.at[index])
            layer2(group, e)
            waiting.append((group, e))
            if len(waiting) > 1:
                reduce_any(*waiting.pop(0))
    for item in waiting:
        reduce_any(*item)
    for e in late:
        finish_late(e)

    for cond, copy in pending:
        if cond is None:
            copy.wait_send()
        else:
            pl.when(cond)(copy.wait_send)
    for e in range(E):
        for zd in range(Z):
            if e in late:
                for y2 in range(Y):
                    pl.when(zd > z)(late_copy(zd, y2, e, True).wait_send)
                    pl.when(zd < z)(late_copy(zd, y2, e, False).wait_send)
            else:
                for o in range(1, Y):
                    cross_copy(zd, o, e).wait_send()
                pl.when(zd > z)(line_copy(zd, e, True).wait_send)
                pl.when(zd < z)(line_copy(zd, e, False).wait_send)
    for e in late:
        for o in range(1, Y):
            final_cross(o, e).wait_send()


def shards(dims, tokens, norm_gain, up_weight, down_weight):
    G, n, T = dims
    Z, Y = line_shape(n)
    rows, cols = up_weight.shape
    here, w = tokens.shape
    deep, dcols = down_weight.shape
    unit = cols * G * T // n
    k = n // (G * T)
    E = 4 if here % 128 == 0 else 1
    early = (E - 1,) if Y == 2 and E > 1 else ()
    late = (0,) if Y == 2 and E > 1 else ()
    width = rows * n
    feat = dcols * G * T // n
    slab = here // E
    L = max(len(late), 1)
    sends = E * (Y + 1) + 2 * k * G + 2 * G + G * T + 2 * Z * Y * (E + 1) * 2 + 2 * Z * Y * G * T + 2 * Z * E * Y
    bf = jnp.bfloat16
    dma = pltpu.SemaphoreType.DMA
    vmem = pl.BlockSpec(memory_space=pltpu.VMEM)
    hbm = pl.BlockSpec(memory_space=pltpu.HBM)
    return pl.pallas_call(
        functools.partial(kernel, G, n, T, Z, Y, k, E, early, late, sends),
        out_shape=(
            pltpu.VMEM((feat, here), bf),
            pltpu.VMEM((width, unit), bf),
            pltpu.VMEM((deep, dcols * G * T), bf),
        ),
        in_specs=[hbm] * 4,
        out_specs=(vmem, vmem, vmem),
        scratch_shapes=[
            pltpu.VMEM((rows, cols), jnp.float32),
            pltpu.VMEM((deep, dcols), jnp.float32),
            pltpu.VMEM((1, rows), jnp.float32),
            pltpu.VMEM((rows, 128), jnp.float32),
            pltpu.VMEM((k, rows, unit), bf),
            pltpu.VMEM((G, k, rows // G, unit), bf),
            pltpu.VMEM((n, here, w), bf),
            pltpu.VMEM((here, unit), bf),
            pltpu.VMEM((n, here, feat), bf),
            pltpu.VMEM((Z, Y, here, feat), bf),
            pltpu.VMEM((Z, here, feat), bf),
            pltpu.VMEM((Z, here, feat), bf),
            pltpu.VMEM((Z, Y, L * slab, feat), bf),
            pltpu.VMEM((Z, Y, L * slab, feat), bf),
            pltpu.VMEM((Y, L * slab, feat), bf),
            dma((G + 2,)), pltpu.SemaphoreType.REGULAR((max(Z - 1, 1),)), dma((sends,)),
            dma((n, E)), dma((k, G)), dma((n, G)), dma((G * T,)),
            dma((Z, Y, E)), dma((Z, E)), dma((Z, E)), dma((Z, Y, L)), dma((Z, Y, L)), dma((2, Y, L)),
            dma((Z, Y, E)), dma((Z, E)), dma((Z, E)), dma((Z, Y, L)), dma((Z, Y, L)),
        ],
        compiler_params=pltpu.CompilerParams(
            collective_id=0, has_side_effects=True, vmem_limit_bytes=52 * 1024 * 1024
        ),
    )(tokens, norm_gain[None, :], up_weight, down_weight)


def solution(mesh):
    dims = (mesh.shape["gr"], mesh.shape["fs"], mesh.shape["tp"])
    in_specs = (P(("gr", "tp"), "fs"), P("fs"), P("fs", ("gr", "tp")), P("fs", ("gr", "tp")))
    out_specs = (P("fs", ("gr", "tp")), P(None, "fs"), P("fs", None))
    return jax.shard_map(
        functools.partial(shards, dims), mesh=mesh, in_specs=in_specs, out_specs=out_specs, check_vma=False
    )
```

time: 141 us -> 171 us (1.21)
  the two profiles are of different devices: /device:TPU:0 before, /device:TPU:6 now
where the time goes in v1:
time: 171 us
  Pallas kernels  166 us (97%)
  local copies, waits for them, and re-layouts  4.82 us (3%)
    pallas_call x1, Pallas kernels, shards(): pl.pallas_call(functools.partial(kernel, G, n, T, Z, Y, k, E, early, late...  166 us
    unnamed x3, local copies, waits for them, and re-layouts  4.82 us

profile of v1, /device:TPU:6, one launch (start us, length us, event | category | flops | bytes accessed | tf_op | source)
XLA Modules:
  0.0 171.1 jit_solution(8122497083014171445)
XLA Ops:
  0.6 165.6 %shard_map.67 = (bf16[256,1024]{1,0:T(8,128)(2,1)S(1)}, bf16[2048,1024]{1,0:T(8,128)(2,1)S(1)}, bf16[1024,2048]{1,0:T(8,128)(2,1)S(1)}) custom-call(bf16[1024,256]{1,0:T(8,128)(2,1)} %tok_ref.1, f32[1,256]{1,0:T(1,128)} %bitcast.1, f32[256,2048]{1,0:T(8,128)} %upw_ref.1, f32[1024,512]{1,0:T(8,128)} %dnw_ref.1), custom_call_target="tpu_custom_call" | custom-call | tf_op jit(solution)/shard_map/pallas_call | solution.py:535
  166.2 0.8 copy.10
  167.0 2.0 %copy.11 = bf16[2048,1024]{1,0:T(8,128)(2,1)} copy(bf16[2048,1024]{1,0:T(8,128)(2,1)S(1)} %get-tuple-element.4) | data formatting | bytes 8388608
  169.1 2.0 %copy.12 = bf16[1024,2048]{1,0:T(8,128)(2,1)} copy(bf16[1024,2048]{1,0:T(8,128)(2,1)S(1)} %get-tuple-element.5) | data formatting | bytes 8388608

commit v2 on v1

v2 whole, which is shorter than its diff:
```python
import functools

import jax
import jax.numpy as jnp
from jax import lax
from jax.experimental import pallas as pl
from jax.experimental.pallas import tpu as pltpu
from jax.sharding import PartitionSpec as P

MESH = pl.DeviceIdType.MESH
epsilon = 1e-06


def line_shape(count):
    short = max(d for d in range(1, count + 1) if count % d == 0 and d * d <= count)
    return count // short, short


def chunks(total, size):
    return min(total, size)


def plan(Z, E, k):
    steps = [("exchange",), ("share", 0), ("down",), ("down across",), ("greet", 0), ("convert",)]
    steps += [("greet", i) for i in range(1, Z)]
    steps += [("owned",), ("share", 1)]
    steps += [("pass", j) for j in range(k)] + [("share", e) for e in range(2, E)]
    steps += [("direct", 0)] + [("tokens", 1, e) for e in range(E)]
    steps += [("direct", 1)] + [("tokens", 2, e) for e in range(E)]
    steps += [("direct", 2)] + [("direct", 3)] + [("tokens", 3, e) for e in range(E)]
    steps += [("far", s) for s in range(Z)]
    return steps

def kernel(
    G, n, T, Z, Y, k, E, C, LAG, INNER, early, send_count,
    tok_ref, gain_ref, upw_ref, dnw_ref,
    mixed_ref, up_full, dn_full,
    upw_v, dnw_v, gain_v, gain_col, up_bf, xbuf, tok_full, hidden, part,
    ybuf, zup, zdn,
    load_sem, hand, send_sem, tok_recv, x_recv, up_recv, dn_recv,
    y_recv, zu_recv, zd_recv, dn_send, y_send, zu_send, zd_send,
):
    g, f, t = lax.axis_index("gr"), lax.axis_index("fs"), lax.axis_index("tp")
    z, y = f // Y, f % Y
    q = g * T + t
    rows = upw_v.shape[0]
    sub = rows // G
    unit = up_full.shape[1]
    dcols = dnw_v.shape[1]
    feat = part.shape[2]
    here = tok_full.shape[1]
    slab = here // E
    per = G * T // Z
    pending = []

    def nth(i):
        value = 0 * z
        for zv in range(Z):
            order = sorted(range(Z), key=lambda zd: (-abs(zd - zv), zd))
            for o in range(Z):
                value = jnp.where((z == zv) & (i == o), order[o], value)
        return value

    def fresh():
        assert len(pending) < send_count
        return send_sem.at[len(pending)]

    def send(src, dst, rsem, dev, cond=None):
        copy = pltpu.make_async_remote_copy(
            src_ref=src, dst_ref=dst, send_sem=fresh(), recv_sem=rsem, device_id=dev, device_id_type=MESH
        )
        if cond is None:
            copy.start()
        else:
            pl.when(cond)(copy.start)
        pending.append((cond, copy))

    def arrived(ref, sem, cond=None):
        wait = pltpu.make_async_copy(ref, ref, sem).wait
        if cond is None:
            wait()
        else:
            pl.when(cond)(wait)

    def tok(c, e):
        return tok_full.at[c, pl.ds(e * slab, slab)]

    loads = []
    for e in range(E):
        loads.append(pltpu.make_async_copy(tok_ref.at[pl.ds(e * slab, slab)], tok(f, e), tok_recv.at[f, e]))
    loads.append(pltpu.make_async_copy(gain_ref, gain_v, load_sem.at[0]))
    for h in range(G):
        r = pl.ds(h * sub, sub)
        loads.append(pltpu.make_async_copy(upw_ref.at[r], upw_v.at[r], load_sem.at[1 + h]))
    loads.append(pltpu.make_async_copy(dnw_ref, dnw_v, load_sem.at[1 + G]))

    barrier = pltpu.get_barrier_semaphore()
    below, above = z > 0, z < Z - 1
    line = below.astype(jnp.int32) + above.astype(jnp.int32)

    def greet(sem, wide):
        def tell(dev):
            pl.semaphore_signal(sem, inc=1, device_id=dev, device_id_type=MESH)

        pl.when(above)(lambda: tell((g, f + Y, t)))
        pl.when(below)(lambda: tell((g, f - Y, t)))
        for o in range(1, Y):
            tell((g, z * Y + (y + o) % Y, t))
        if wide:
            for o in range(1, G):
                tell(((g + o) % G, f, t))
            for o in range(1, T):
                tell((g, f, (t + o) % T))

    greet(barrier, True)
    for copy in loads:
        copy.start()
    pl.semaphore_wait(barrier, line + (Y - 1) + (G - 1) + (T - 1))

    rounds = Z
    greeted = [0]

    def next_round():
        if greeted[0] < rounds:
            greet(hand.at[greeted[0]], False)
            greeted[0] += 1

    def round_over(i):
        if i < rounds:
            pl.semaphore_wait(hand.at[i], line + (Y - 1))

    next_round()

    for copy in loads[E:E + 1]:
        copy.wait()
    wide_gain = jnp.broadcast_to(gain_v[...], (128, rows))
    gain_col[...] = wide_gain.T

    step = chunks(sub, 32)

    def convert_up(h):
        @pl.loop(0, sub // step)
        def _(i):
            r = pl.ds(pl.multiple_of(h * sub + i * step, step), step)
            column = gain_col[r, 0:1]
            for j in range(k):
                up_bf[j, r, :] = (column * upw_v[r, pl.ds(j * unit, unit)]).astype(jnp.bfloat16)

    def piece(c, h):
        return up_full.at[pl.ds(pl.multiple_of(c * rows + h * sub, sub), sub)]

    def half(j, h):
        return up_bf.at[j, pl.ds(pl.multiple_of(h * sub, sub), sub)]

    def share_tokens(e):
        loads[e].wait()
        own = tok(f, e)
        for o in range(1, Y):
            send(own, own, tok_recv.at[f, e], (g, z * Y + (y + o) % Y, t))
        send(own, own, tok_recv.at[f, e], (g, f + Y, t), above)
        send(own, own, tok_recv.at[f, e], (g, f - Y, t), below)

    def start_exchange():
        for oh in range(1, G):
            h = (g + oh) % G
            convert_up(h)
            for j in range(k):
                send(half(j, h), xbuf.at[G - oh, j], x_recv.at[j, G - oh], (h, f, t))

    relay_core = f % T

    def to_owner(j, source_q, src):
        owner = source_q * k + j
        local = pltpu.make_async_copy(src, piece(f, g), up_recv.at[f, g])
        stays = (owner == f) & (relay_core == t)
        pl.when(stays)(local.start)
        send(src, piece(f, g), up_recv.at[f, g], (g, owner, relay_core), jnp.logical_not(stays))

    def start_owned():
        for j in range(k):
            to_owner(j, q, half(j, g))

    deep = dnw_v.shape[0]
    drows = deep // C

    def dn_block(index, i):
        return dn_full.at[pl.ds(i * drows, drows), pl.ds(pl.multiple_of(index * dcols, dcols), dcols)]

    dstep = chunks(deep, 64)

    def start_down():
        loads[E + 1 + G].wait()

        @pl.loop(0, deep // dstep)
        def _(i):
            r = pl.ds(pl.multiple_of(i * dstep, dstep), dstep)
            dn_full[r, pl.ds(pl.multiple_of(q * dcols, dcols), dcols)] = dnw_v[r, :].astype(jnp.bfloat16)

        for i in range(C):
            for o in range(1, T):
                send(dn_block(q, i), dn_block(q, i), dn_recv.at[q, i], (g, f, (t + o) % T))


    def down_across():
        for i in range(C):
            for o in range(1, G):
                send(dn_block(q, i), dn_block(q, i), dn_recv.at[q, i], ((g + o) % G, f, t))

    def relay_direct(c, cond):
        ok = (c % T == t) & cond
        arrived(piece(c, g), up_recv.at[c, g], ok)
        for o in range(1, G):
            send(piece(c, g), piece(c, g), up_recv.at[c, g], ((g + o) % G, f, t), ok)
        for o in range(1, T):
            send(piece(c, g), piece(c, g), up_recv.at[c, g], (g, f, (t + o) % T), ok)

    def relay_far(c, cond):
        ok = (c % T == t) & cond
        for oh in range(1, G):
            h = (g + oh) % G
            arrived(piece(c, h), up_recv.at[c, h], ok)
            for o in range(1, T):
                send(piece(c, h), piece(c, h), up_recv.at[c, h], (g, f, (t + o) % T), ok)

    def on_tokens(c, e, cond, up, down, cross):
        arrived(tok(c, e), tok_recv.at[c, e], cond)
        if up is not None:
            send(tok(c, e), tok(c, e), tok_recv.at[c, e], (g, f + Y, t), up)
        if down is not None:
            send(tok(c, e), tok(c, e), tok_recv.at[c, e], (g, f - Y, t), down)
        if cross:
            for o in range(1, Y):
                send(tok(c, e), tok(c, e), tok_recv.at[c, e], (g, z * Y + (y + o) % Y, t), cond)

    def from_exchange(j):
        for og in range(1, G):
            arrived(xbuf.at[og, j], x_recv.at[j, og])
            to_owner(j, ((g + og) % G) * T + t, xbuf.at[og, j])

    def pieces_at(s):
        if s == 0:
            return [(z * Y + (y + o) % Y, True) for o in range(Y)]
        lower, upper = z - s >= 0, z + s < Z
        zl, zu = jnp.maximum(z - s, 0), jnp.minimum(z + s, Z - 1)
        found = []
        for o in range(Y):
            found.append((zl * Y + (y + o) % Y, lower))
            found.append((zu * Y + (y + o) % Y, upper))
        return found

    def tokens_at(s, e):
        if s == 0:
            if e in early:
                for o in range(1, Y):
                    on_tokens(z * Y + (y + o) % Y, e, None, above, below, False)
            return
        lower, upper = z - s >= 0, z + s < Z
        zl, zu = jnp.maximum(z - s, 0), jnp.minimum(z + s, Z - 1)
        if e in early:
            for o in range(Y):
                y2 = (y + o) % Y
                on_tokens(zl * Y + y2, e, lower, lower & above, None, False)
                on_tokens(zu * Y + y2, e, upper, None, upper & below, False)
        else:
            on_tokens(zl * Y + y, e, lower, lower & above, None, True)
            on_tokens(zu * Y + y, e, upper, None, upper & below, True)

    def greet_round(i):
        round_over(i)
        next_round()

    def on_pieces(s, relay):
        for c, cond in pieces_at(s):
            relay(c, cond)

    for copy in loads[E + 1:E + 1 + G]:
        copy.wait()
    for step_name in plan(Z, E, k):
        kind, *at = step_name
        {
            "share": share_tokens, "exchange": start_exchange, "convert": lambda: convert_up(g), "greet": greet_round,
            "owned": start_owned, "pass": from_exchange, "tokens": tokens_at, "down": start_down,
            "down across": down_across,
            "direct": lambda s: on_pieces(s, relay_direct), "far": lambda s: on_pieces(s, relay_far),
        }[kind](*at)

    @pl.loop(0, n)
    def _(c):
        for h in range(G):
            arrived(piece(c, h), up_recv.at[c, h], c % T != t)

    width = n * tok_full.shape[2]

    def span(e):
        return pl.ds(pl.multiple_of(e * slab, slab), slab)

    def layer1(e):
        r = span(e)
        crossed_late = e >= 0
        for other in early:
            crossed_late = crossed_late & (e != other)

        @pl.when(crossed_late)
        def _():
            for zc in range(Z):
                for o in range(1, Y):
                    c = zc * Y + (y + o) % Y
                    arrived(tok_full.at[c, r], tok_recv.at[c, e])
        blocks = [tok_full[c, r, :] for c in range(n)]
        squares = None
        for block in blocks:
            wide = block.astype(jnp.float32)
            total = jnp.sum(wide * wide, axis=1, keepdims=True)
            squares = total if squares is None else squares + total
        scale = lax.rsqrt(squares / width + epsilon)
        raw = jnp.dot(jnp.concatenate(blocks, axis=1), up_full[...], preferred_element_type=jnp.float32)
        hidden[r, :] = jnp.square(jnp.maximum(raw * scale, 0.0)).astype(jnp.bfloat16)

    def cross_copy(zd, o, e):
        y2 = (y + o) % Y
        return pltpu.make_async_remote_copy(
            src_ref=part.at[zd * Y + y2, span(e)], dst_ref=ybuf.at[zd, Y - o, span(e)], send_sem=y_send.at[zd, o, e],
            recv_sem=y_recv.at[zd, Y - o, e], device_id=(g, z * Y + y2, t), device_id_type=MESH,
        )

    def line_copy(zd, e, up):
        c = zd * Y + y
        if up:
            return pltpu.make_async_remote_copy(
                src_ref=part.at[c, span(e)], dst_ref=zup.at[zd, span(e)], send_sem=zu_send.at[zd, e],
                recv_sem=zu_recv.at[zd, e], device_id=(g, f + Y, t), device_id_type=MESH,
            )
        return pltpu.make_async_remote_copy(
            src_ref=part.at[c, span(e)], dst_ref=zdn.at[zd, span(e)], send_sem=zd_send.at[zd, e],
            recv_sem=zd_recv.at[zd, e], device_id=(g, f - Y, t), device_id_type=MESH,
        )

    def layer2(i, e):
        r = span(e)
        zd = nth(i)
        cols = dn_full[:, pl.ds(pl.multiple_of(zd * (Y * feat), Y * feat), Y * feat)]
        whole = jnp.dot(hidden[r, :], cols, preferred_element_type=jnp.float32).astype(jnp.bfloat16)
        for y2 in range(Y):
            part[zd * Y + y2, r, :] = whole[:, y2 * feat:(y2 + 1) * feat]
        for o in range(1, Y):
            cross_copy(zd, o, e).start()

    rstep = chunks(slab, 32)
    fstep = chunks(slab, 128)

    def add_up(c, e, extras, final=False):
        size = fstep if final else rstep

        @pl.loop(0, slab // size)
        def _(i):
            r = pl.ds(pl.multiple_of(e * slab + i * size, size), size)
            total = part[c, r, :].astype(jnp.float32)
            for ref, base in extras:
                total = total + ref[pl.ds(pl.multiple_of(base + i * size, size), size), :].astype(jnp.float32)
            if final:
                mixed_ref[:, r] = total.T.astype(jnp.bfloat16)
            else:
                part[c, r, :] = total.astype(jnp.bfloat16)

    ends = [
        (jnp.bool_(True), False, False) if Z == 1 else (z == 0, False, True),
    ]
    if Z > 1:
        ends.append((z == Z - 1, True, False))
    if Z > 2:
        ends.append((below & above, True, True))

    def finish(e, low, high, crossed):
        for cond, has_low, has_high in ends:
            extras = list(crossed) + ([low] if has_low else []) + ([high] if has_high else [])

            @pl.when(cond)
            def _():
                add_up(z * Y + y, e, extras, True)

    def add_step(index):
        held = jnp.clip(index, 0, items - 1)
        zd, e = nth(held // E), held % E
        go = (index >= 0) & (index < items)
        going_up, going_down = go & (zd > z), go & (zd < z)
        c = zd * Y + y
        base = e * slab
        crossed = [(ybuf.at[zd, o], base) for o in range(1, Y)]
        low, high = (zup.at[zd], base), (zdn.at[zd], base)
        for o in range(1, Y):
            arrived(ybuf.at[zd, o, span(e)], y_recv.at[zd, o, e], go)
        arrived(zup.at[zd, span(e)], zu_recv.at[zd, e], go & (zd >= z) & below)
        arrived(zdn.at[zd, span(e)], zd_recv.at[zd, e], go & (zd <= z) & above)
        if crossed:
            pl.when((going_up & (z == 0)) | (going_down & (z == Z - 1)))(lambda: add_up(c, e, crossed))
        pl.when(going_up & below)(lambda: add_up(c, e, crossed + [low]))
        pl.when(going_down & above)(lambda: add_up(c, e, crossed + [high]))
        pl.when(going_up)(lambda: line_copy(zd, e, True).start())
        pl.when(going_down)(lambda: line_copy(zd, e, False).start())
        pl.when(go & (zd == z))(lambda: finish(e, low, high, crossed))

    def down_over(b, o, i):
        return pltpu.make_async_remote_copy(
            src_ref=dn_block(b, i), dst_ref=dn_block(b, i), send_sem=dn_send.at[b, o, i],
            recv_sem=dn_recv.at[b, i], device_id=(g, f, (t + o) % T), device_id_type=MESH,
        )

    def down_forward(i):
        zd = nth(i)
        for at in range(per):
            b = zd * per + at

            @pl.when((b // T != g) & (b % T == t))
            def _():
                for part_of in range(C):
                    arrived(dn_block(b, part_of), dn_recv.at[b, part_of])
                    for o in range(1, T):
                        down_over(b, o, part_of).start()

    def down_wait(i):
        zd = nth(i)
        for at in range(per):
            b = zd * per + at

            @pl.when(b % T != t)
            def _():
                for part_of in range(C):
                    arrived(dn_block(b, part_of), dn_recv.at[b, part_of])

    items = Z * E
    delay = LAG + jnp.where(below & above, INNER, 0)
    down_forward(0)

    @pl.loop(0, items + LAG + INNER)
    def _(stage):
        @pl.when(stage < items)
        def _():
            i, e = stage // E, stage % E
            pl.when(i == 0)(lambda: layer1(e))
            pl.when((e == E - 1) & (i < Z - 1))(lambda: down_forward(i + 1))
            pl.when(e == 0)(lambda: down_wait(i))
            layer2(i, e)

        add_step(stage - delay)

    for cond, copy in pending:
        if cond is None:
            copy.wait_send()
        else:
            pl.when(cond)(copy.wait_send)
    for e in range(E):
        for zd in range(Z):
            for o in range(1, Y):
                cross_copy(zd, o, e).wait_send()
            pl.when(zd > z)(line_copy(zd, e, True).wait_send)
            pl.when(zd < z)(line_copy(zd, e, False).wait_send)
    for b in range(G * T):
        for o in range(1, T):
            for i in range(C):
                pl.when((b // T != g) & (b % T == t))(down_over(b, o, i).wait_send)


def shards(dims, tokens, norm_gain, up_weight, down_weight):
    G, n, T = dims
    Z, Y = line_shape(n)
    rows, cols = up_weight.shape
    here, w = tokens.shape
    deep, dcols = down_weight.shape
    unit = cols * G * T // n
    k = n // (G * T)
    E = 4 if here % 128 == 0 else 1
    early = () if Y == 2 and E > 1 else ()
    C, LAG, INNER = 4, 2, 2
    width = rows * n
    feat = dcols * G * T // n
    sends = E * (Y + 1) + 2 * k * G + 2 * C * G * T + 2 * Z * Y * (E + 1) * 2 + 2 * Z * Y * G * T + 2 * Z * E * Y
    bf = jnp.bfloat16
    dma = pltpu.SemaphoreType.DMA
    vmem = pl.BlockSpec(memory_space=pltpu.VMEM)
    hbm = pl.BlockSpec(memory_space=pltpu.HBM)
    return pl.pallas_call(
        functools.partial(kernel, G, n, T, Z, Y, k, E, C, LAG, INNER, early, sends),
        out_shape=(
            pltpu.VMEM((feat, here), bf),
            pltpu.VMEM((width, unit), bf),
            pltpu.VMEM((deep, dcols * G * T), bf),
        ),
        in_specs=[hbm] * 4,
        out_specs=(vmem, vmem, vmem),
        scratch_shapes=[
            pltpu.VMEM((rows, cols), jnp.float32),
            pltpu.VMEM((deep, dcols), jnp.float32),
            pltpu.VMEM((1, rows), jnp.float32),
            pltpu.VMEM((rows, 128), jnp.float32),
            pltpu.VMEM((k, rows, unit), bf),
            pltpu.VMEM((G, k, rows // G, unit), bf),
            pltpu.VMEM((n, here, w), bf),
            pltpu.VMEM((here, unit), bf),
            pltpu.VMEM((n, here, feat), bf),
            pltpu.VMEM((Z, Y, here, feat), bf),
            pltpu.VMEM((Z, here, feat), bf),
            pltpu.VMEM((Z, here, feat), bf),
            dma((G + 2,)), pltpu.SemaphoreType.REGULAR((Z,)), dma((sends,)),
            dma((n, E)), dma((k, G)), dma((n, G)), dma((G * T, C)),
            dma((Z, Y, E)), dma((Z, E)), dma((Z, E)), dma((G * T, T, C)), dma((Z, Y, E)), dma((Z, E)), dma((Z, E)),
        ],
        compiler_params=pltpu.CompilerParams(
            collective_id=0, has_side_effects=True, vmem_limit_bytes=52 * 1024 * 1024
        ),
    )(tokens, norm_gain[None, :], up_weight, down_weight)


def solution(mesh):
    dims = (mesh.shape["gr"], mesh.shape["fs"], mesh.shape["tp"])
    in_specs = (P(("gr", "tp"), "fs"), P("fs"), P("fs", ("gr", "tp")), P("fs", ("gr", "tp")))
    out_specs = (P("fs", ("gr", "tp")), P(None, "fs"), P("fs", None))
    return jax.shard_map(
        functools.partial(shards, dims), mesh=mesh, in_specs=in_specs, out_specs=out_specs, check_vma=False
    )
```

time: 171 us -> 124 us (0.73)
  the two profiles are of different devices: /device:TPU:6 before, /device:TPU:0 now
where the time goes in v2:
time: 124 us
  Pallas kernels  119 us (96%)
  local copies, waits for them, and re-layouts  4.82 us (4%)
    pallas_call x1, Pallas kernels, shards(): pl.pallas_call(functools.partial(kernel, G, n, T, Z, Y, k, E, C, LAG, INN...  119 us
    unnamed x3, local copies, waits for them, and re-layouts  4.82 us

profile of v2, /device:TPU:0, one launch (start us, length us, event | category | flops | bytes accessed | tf_op | source)
XLA Modules:
  0.0 124.0 jit_solution(6437802057004726404)
XLA Ops:
  0.6 118.6 %shard_map.67 = (bf16[256,1024]{1,0:T(8,128)(2,1)S(1)}, bf16[2048,1024]{1,0:T(8,128)(2,1)S(1)}, bf16[1024,2048]{1,0:T(8,128)(2,1)S(1)}) custom-call(bf16[1024,256]{1,0:T(8,128)(2,1)} %tok_ref.1, f32[1,256]{1,0:T(1,128)} %bitcast.1, f32[256,2048]{1,0:T(8,128)} %upw_ref.1, f32[1024,512]{1,0:T(8,128)} %dnw_ref.1), custom_call_target="tpu_custom_call" | custom-call | tf_op jit(solution)/shard_map/pallas_call | solution.py:481
  119.2 0.8 copy.10
  120.0 2.0 %copy.11 = bf16[2048,1024]{1,0:T(8,128)(2,1)} copy(bf16[2048,1024]{1,0:T(8,128)(2,1)S(1)} %get-tuple-element.4) | data formatting | bytes 8388608
  122.0 2.0 %copy.12 = bf16[1024,2048]{1,0:T(8,128)(2,1)} copy(bf16[1024,2048]{1,0:T(8,128)(2,1)S(1)} %get-tuple-element.5) | data formatting | bytes 8388608

commit v3 on v2

--- a/solution.py
+++ b/solution.py
@@ -20,19 +20,23 @@
     return min(total, size)
 
 
-def plan(Z, E, k):
-    steps = [("exchange",), ("share", 0), ("down",), ("down across",), ("greet", 0), ("convert",)]
-    steps += [("greet", i) for i in range(1, Z)]
-    steps += [("owned",), ("share", 1)]
-    steps += [("pass", j) for j in range(k)] + [("share", e) for e in range(2, E)]
-    steps += [("direct", 0)] + [("tokens", 1, e) for e in range(E)]
-    steps += [("direct", 1)] + [("tokens", 2, e) for e in range(E)]
-    steps += [("direct", 2)] + [("direct", 3)] + [("tokens", 3, e) for e in range(E)]
-    steps += [("far", s) for s in range(Z)]
+def plan(Z, B, k, S, C):
+    early = C // 2
+    steps = [("exchange",), ("share", 0), ("down",), ("down across", 0, C, True), ("down across", 0, early, False)]
+    steps += [("greet", i) for i in range(Z)]
+    steps += [("owned",)] + [("share", e) for e in range(1, B)]
+    steps += [("pass", j, s) for s in range(S) for j in range(k)]
+    for far in range(Z - 1):
+        steps += [("direct", far, s) for s in range(S)]
+        if far + 2 == Z:
+            steps += [("direct", Z - 1, s) for s in range(S)] + [("down across", early, C, False)]
+        steps += [("tokens", far + 1, e) for e in range(B)]
+    steps += [("far", far, s) for s in range(S) for far in range(Z)]
     return steps
 
+
 def kernel(
-    G, n, T, Z, Y, k, E, C, LAG, INNER, early, send_count,
+    G, n, T, Z, Y, k, E, B, S, C, LAG, INNER, send_count,
     tok_ref, gain_ref, upw_ref, dnw_ref,
     mixed_ref, up_full, dn_full,
     upw_v, dnw_v, gain_v, gain_col, up_bf, xbuf, tok_full, hidden, part,
@@ -50,6 +54,7 @@
     feat = part.shape[2]
     here = tok_full.shape[1]
     slab = here // E
+    batch = here // B
     per = G * T // Z
     pending = []
 
@@ -83,11 +88,11 @@
             pl.when(cond)(wait)
 
     def tok(c, e):
-        return tok_full.at[c, pl.ds(e * slab, slab)]
+        return tok_full.at[c, pl.ds(e * batch, batch)]
 
     loads = []
-    for e in range(E):
-        loads.append(pltpu.make_async_copy(tok_ref.at[pl.ds(e * slab, slab)], tok(f, e), tok_recv.at[f, e]))
+    for e in range(B):
+        loads.append(pltpu.make_async_copy(tok_ref.at[pl.ds(e * batch, batch)], tok(f, e), tok_recv.at[f, e]))
     loads.append(pltpu.make_async_copy(gain_ref, gain_v, load_sem.at[0]))
     for h in range(G):
         r = pl.ds(h * sub, sub)
@@ -112,10 +117,9 @@
             for o in range(1, T):
                 tell((g, f, (t + o) % T))
 
+    for at in list(range(B, B + 1 + G)) + list(range(B)) + [B + 1 + G]:
+        loads[at].start()
     greet(barrier, True)
-    for copy in loads:
-        copy.start()
-    pl.semaphore_wait(barrier, line + (Y - 1) + (G - 1) + (T - 1))
 
     rounds = Z
     greeted = [0]
@@ -129,10 +133,7 @@
         if i < rounds:
             pl.semaphore_wait(hand.at[i], line + (Y - 1))
 
-    next_round()
-
-    for copy in loads[E:E + 1]:
-        copy.wait()
+    loads[B].wait()
     wide_gain = jnp.broadcast_to(gain_v[...], (128, rows))
     gain_col[...] = wide_gain.T
 
@@ -146,11 +147,13 @@
             for j in range(k):
                 up_bf[j, r, :] = (column * upw_v[r, pl.ds(j * unit, unit)]).astype(jnp.bfloat16)
 
-    def piece(c, h):
-        return up_full.at[pl.ds(pl.multiple_of(c * rows + h * sub, sub), sub)]
-
-    def half(j, h):
-        return up_bf.at[j, pl.ds(pl.multiple_of(h * sub, sub), sub)]
+    bit = sub // S
+
+    def piece(c, h, s):
+        return up_full.at[pl.ds(pl.multiple_of(c * rows + h * sub + s * bit, bit), bit)]
+
+    def half(j, h, s):
+        return up_bf.at[j, pl.ds(pl.multiple_of(h * sub + s * bit, bit), bit)]
 
     def share_tokens(e):
         loads[e].wait()
@@ -160,25 +163,29 @@
         send(own, own, tok_recv.at[f, e], (g, f + Y, t), above)
         send(own, own, tok_recv.at[f, e], (g, f - Y, t), below)
 
+    def xpart(og, j, s):
+        return xbuf.at[og, j, pl.ds(s * bit, bit)]
+
     def start_exchange():
         for oh in range(1, G):
             h = (g + oh) % G
-            convert_up(h)
-            for j in range(k):
-                send(half(j, h), xbuf.at[G - oh, j], x_recv.at[j, G - oh], (h, f, t))
+            for s in range(S):
+                for j in range(k):
+                    send(half(j, h, s), xpart(G - oh, j, s), x_recv.at[j, G - oh, s], (h, f, t))
 
     relay_core = f % T
 
-    def to_owner(j, source_q, src):
+    def to_owner(j, s, source_q, src):
         owner = source_q * k + j
-        local = pltpu.make_async_copy(src, piece(f, g), up_recv.at[f, g])
+        local = pltpu.make_async_copy(src, piece(f, g, s), up_recv.at[f, g, s])
         stays = (owner == f) & (relay_core == t)
         pl.when(stays)(local.start)
-        send(src, piece(f, g), up_recv.at[f, g], (g, owner, relay_core), jnp.logical_not(stays))
+        send(src, piece(f, g, s), up_recv.at[f, g, s], (g, owner, relay_core), jnp.logical_not(stays))
 
     def start_owned():
-        for j in range(k):
-            to_owner(j, q, half(j, g))
+        for s in range(S):
+            for j in range(k):
+                to_owner(j, s, q, half(j, g, s))
 
     deep = dnw_v.shape[0]
     drows = deep // C
@@ -189,7 +196,7 @@
     dstep = chunks(deep, 64)
 
     def start_down():
-        loads[E + 1 + G].wait()
+        loads[B + 1 + G].wait()
 
         @pl.loop(0, deep // dstep)
         def _(i):
@@ -201,41 +208,41 @@
                 send(dn_block(q, i), dn_block(q, i), dn_recv.at[q, i], (g, f, (t + o) % T))
 
 
-    def down_across():
-        for i in range(C):
+    def down_across(first, last, near=None):
+        cond = None if near is None else ((nth(0) == q // per) == near)
+        for i in range(first, last):
             for o in range(1, G):
-                send(dn_block(q, i), dn_block(q, i), dn_recv.at[q, i], ((g + o) % G, f, t))
-
-    def relay_direct(c, cond):
+                send(dn_block(q, i), dn_block(q, i), dn_recv.at[q, i], ((g + o) % G, f, t), cond)
+
+    def relay_direct(c, s, cond):
         ok = (c % T == t) & cond
-        arrived(piece(c, g), up_recv.at[c, g], ok)
+        arrived(piece(c, g, s), up_recv.at[c, g, s], ok)
         for o in range(1, G):
-            send(piece(c, g), piece(c, g), up_recv.at[c, g], ((g + o) % G, f, t), ok)
+            send(piece(c, g, s), piece(c, g, s), up_recv.at[c, g, s], ((g + o) % G, f, t), ok)
         for o in range(1, T):
-            send(piece(c, g), piece(c, g), up_recv.at[c, g], (g, f, (t + o) % T), ok)
-
-    def relay_far(c, cond):
+            send(piece(c, g, s), piece(c, g, s), up_recv.at[c, g, s], (g, f, (t + o) % T), ok)
+
+    def relay_far(c, s, cond):
         ok = (c % T == t) & cond
         for oh in range(1, G):
             h = (g + oh) % G
-            arrived(piece(c, h), up_recv.at[c, h], ok)
+            arrived(piece(c, h, s), up_recv.at[c, h, s], ok)
             for o in range(1, T):
-                send(piece(c, h), piece(c, h), up_recv.at[c, h], (g, f, (t + o) % T), ok)
-
-    def on_tokens(c, e, cond, up, down, cross):
+                send(piece(c, h, s), piece(c, h, s), up_recv.at[c, h, s], (g, f, (t + o) % T), ok)
+
+    def on_tokens(c, e, cond, up, down):
         arrived(tok(c, e), tok_recv.at[c, e], cond)
         if up is not None:
             send(tok(c, e), tok(c, e), tok_recv.at[c, e], (g, f + Y, t), up)
         if down is not None:
             send(tok(c, e), tok(c, e), tok_recv.at[c, e], (g, f - Y, t), down)
-        if cross:
-            for o in range(1, Y):
-                send(tok(c, e), tok(c, e), tok_recv.at[c, e], (g, z * Y + (y + o) % Y, t), cond)
-
-    def from_exchange(j):
+        for o in range(1, Y):
+            send(tok(c, e), tok(c, e), tok_recv.at[c, e], (g, z * Y + (y + o) % Y, t), cond)
+
+    def from_exchange(j, s):
         for og in range(1, G):
-            arrived(xbuf.at[og, j], x_recv.at[j, og])
-            to_owner(j, ((g + og) % G) * T + t, xbuf.at[og, j])
+            arrived(xpart(og, j, s), x_recv.at[j, og, s])
+            to_owner(j, s, ((g + og) % G) * T + t, xpart(og, j, s))
 
     def pieces_at(s):
         if s == 0:
@@ -249,45 +256,39 @@
         return found
 
     def tokens_at(s, e):
-        if s == 0:
-            if e in early:
-                for o in range(1, Y):
-                    on_tokens(z * Y + (y + o) % Y, e, None, above, below, False)
-            return
         lower, upper = z - s >= 0, z + s < Z
         zl, zu = jnp.maximum(z - s, 0), jnp.minimum(z + s, Z - 1)
-        if e in early:
-            for o in range(Y):
-                y2 = (y + o) % Y
-                on_tokens(zl * Y + y2, e, lower, lower & above, None, False)
-                on_tokens(zu * Y + y2, e, upper, None, upper & below, False)
-        else:
-            on_tokens(zl * Y + y, e, lower, lower & above, None, True)
-            on_tokens(zu * Y + y, e, upper, None, upper & below, True)
+        on_tokens(zl * Y + y, e, lower, lower & above, None)
+        on_tokens(zu * Y + y, e, upper, None, upper & below)
 
     def greet_round(i):
         round_over(i)
         next_round()
 
-    def on_pieces(s, relay):
-        for c, cond in pieces_at(s):
-            relay(c, cond)
-
-    for copy in loads[E + 1:E + 1 + G]:
+    def on_pieces(far, s, relay):
+        for c, cond in pieces_at(far):
+            relay(c, s, cond)
+
+    for copy in loads[B + 1:B + 1 + G]:
         copy.wait()
-    for step_name in plan(Z, E, k):
+    for h in range(G):
+        convert_up(h)
+    pl.semaphore_wait(barrier, line + (Y - 1) + (G - 1) + (T - 1))
+    next_round()
+    for step_name in plan(Z, B, k, S, C):
         kind, *at = step_name
         {
-            "share": share_tokens, "exchange": start_exchange, "convert": lambda: convert_up(g), "greet": greet_round,
+            "share": share_tokens, "exchange": start_exchange, "greet": greet_round,
             "owned": start_owned, "pass": from_exchange, "tokens": tokens_at, "down": start_down,
             "down across": down_across,
-            "direct": lambda s: on_pieces(s, relay_direct), "far": lambda s: on_pieces(s, relay_far),
+            "direct": lambda far, s: on_pieces(far, s, relay_direct), "far": lambda far, s: on_pieces(far, s, relay_far),
         }[kind](*at)
 
     @pl.loop(0, n)
     def _(c):
         for h in range(G):
-            arrived(piece(c, h), up_recv.at[c, h], c % T != t)
+            for s in range(S):
+                arrived(piece(c, h, s), up_recv.at[c, h, s], c % T != t)
 
     width = n * tok_full.shape[2]
 
@@ -296,16 +297,15 @@
 
     def layer1(e):
         r = span(e)
-        crossed_late = e >= 0
-        for other in early:
-            crossed_late = crossed_late & (e != other)
-
-        @pl.when(crossed_late)
+        @pl.when(e % (E // B) == 0)
         def _():
             for zc in range(Z):
                 for o in range(1, Y):
                     c = zc * Y + (y + o) % Y
-                    arrived(tok_full.at[c, r], tok_recv.at[c, e])
+                    at = e // (E // B)
+                    rows_in = pl.ds(pl.multiple_of(at * batch, batch), batch)
+                    arrived(tok_full.at[c, rows_in], tok_recv.at[c, at])
+
         blocks = [tok_full[c, r, :] for c in range(n)]
         squares = None
         for block in blocks:
@@ -460,6 +460,19 @@
                 pl.when((b // T != g) & (b % T == t))(down_over(b, o, i).wait_send)
 
 
+def drain(cuts, mixed_in, up_in, dn_in, mixed_out, up_out, dn_out, sems):
+    copies = []
+    for at, (src, dst) in enumerate([(up_in, up_out), (dn_in, dn_out), (mixed_in, mixed_out)]):
+        size = src.shape[0] // cuts
+        for i in range(cuts):
+            r = pl.ds(i * size, size)
+            copies.append(pltpu.make_async_copy(src.at[r], dst.at[r], sems.at[at, i]))
+    for copy in copies:
+        copy.start()
+    for copy in copies:
+        copy.wait()
+
+
 def shards(dims, tokens, norm_gain, up_weight, down_weight):
     G, n, T = dims
     Z, Y = line_shape(n)
@@ -469,17 +482,19 @@
     unit = cols * G * T // n
     k = n // (G * T)
     E = 4 if here % 128 == 0 else 1
-    early = () if Y == 2 and E > 1 else ()
-    C, LAG, INNER = 4, 2, 2
+    B = 2 if E % 2 == 0 else 1
+    S, C, LAG, INNER = 1, 4, 2, 2
     width = rows * n
     feat = dcols * G * T // n
-    sends = E * (Y + 1) + 2 * k * G + 2 * C * G * T + 2 * Z * Y * (E + 1) * 2 + 2 * Z * Y * G * T + 2 * Z * E * Y
+    sends = B * (Y + 1) + 2 * (Z - 1) * B * Y
+    sends += k * (G - 1) * S + k * G * S + C * (T - 1) + 2 * C * (G - 1)
+    sends += (2 * Z - 1) * Y * S * ((G - 1) + G * (T - 1))
     bf = jnp.bfloat16
     dma = pltpu.SemaphoreType.DMA
     vmem = pl.BlockSpec(memory_space=pltpu.VMEM)
     hbm = pl.BlockSpec(memory_space=pltpu.HBM)
-    return pl.pallas_call(
-        functools.partial(kernel, G, n, T, Z, Y, k, E, C, LAG, INNER, early, sends),
+    held = pl.pallas_call(
+        functools.partial(kernel, G, n, T, Z, Y, k, E, B, S, C, LAG, INNER, sends),
         out_shape=(
             pltpu.VMEM((feat, here), bf),
             pltpu.VMEM((width, unit), bf),
@@ -501,13 +516,22 @@
             pltpu.VMEM((Z, here, feat), bf),
             pltpu.VMEM((Z, here, feat), bf),
             dma((G + 2,)), pltpu.SemaphoreType.REGULAR((Z,)), dma((sends,)),
-            dma((n, E)), dma((k, G)), dma((n, G)), dma((G * T, C)),
+            dma((n, B)), dma((k, G, S)), dma((n, G, S)), dma((G * T, C)),
             dma((Z, Y, E)), dma((Z, E)), dma((Z, E)), dma((G * T, T, C)), dma((Z, Y, E)), dma((Z, E)), dma((Z, E)),
         ],
         compiler_params=pltpu.CompilerParams(
             collective_id=0, has_side_effects=True, vmem_limit_bytes=52 * 1024 * 1024
         ),
     )(tokens, norm_gain[None, :], up_weight, down_weight)
+    cuts = 4
+    return pl.pallas_call(
+        functools.partial(drain, cuts),
+        out_shape=tuple(jax.ShapeDtypeStruct(x.shape, bf) for x in held),
+        in_specs=[vmem] * 3,
+        out_specs=(hbm,) * 3,
+        scratch_shapes=[dma((3, cuts))],
+        compiler_params=pltpu.CompilerParams(vmem_limit_bytes=12 * 1024 * 1024),
+    )(*held)
 
 
 def solution(mesh):

time: 124 us -> 118 us (0.952)
  local copies, waits for them, and re-layouts: 4.82 us -> 0 us
  Pallas kernels: 119 us -> 117 us
    unnamed x3 -> x0, local copies, waits for them, and re-layouts: 4.82 us -> none
    pallas_call x1 -> x2, Pallas kernels: 119 us -> 117 us  [the longest x1 114 us: shards(): pl.pallas_call(functools.partial(kernel, G, n, T, Z, Y, k, E, B, S, C, LA...]
where the time goes in v3:
time: 118 us
  Pallas kernels  117 us (99%)
    pallas_call x1, Pallas kernels, shards(): pl.pallas_call(functools.partial(kernel, G, n, T, Z, Y, k, E, B, S, C, LA...  114 us
    pallas_call x1, Pallas kernels, shards(): pl.pallas_call(functools.partial(drain, cuts), out_shape=tuple((jax.Shape...  3.52 us

profile of v3, /device:TPU:0, one launch (start us, length us, event | category | flops | bytes accessed | tf_op | source)
XLA Modules:
  0.0 117.8 jit_solution(1530417290591647732)
XLA Ops:
  0.6 113.6 %shard_map.67 = (bf16[256,1024]{1,0:T(8,128)(2,1)S(1)}, bf16[2048,1024]{1,0:T(8,128)(2,1)S(1)}, bf16[1024,2048]{1,0:T(8,128)(2,1)S(1)}) custom-call(bf16[1024,256]{1,0:T(8,128)(2,1)} %tok_ref.1, f32[1,256]{1,0:T(1,128)} %bitcast.1, f32[256,2048]{1,0:T(8,128)} %upw_ref.1, f32[1024,512]{1,0:T(8,128)} %dnw_ref.1), custom_call_target="tpu_custom_call" | custom-call | tf_op jit(solution)/shard_map/pallas_call | solution.py:496
  114.2 3.5 %shard_map.68 = (bf16[256,1024]{1,0:T(8,128)(2,1)}, bf16[2048,1024]{1,0:T(8,128)(2,1)}, bf16[1024,2048]{1,0:T(8,128)(2,1)}) custom-call(bf16[256,1024]{1,0:T(8,128)(2,1)S(1)} %get-tuple-element.6.mixed_in, bf16[2048,1024]{1,0:T(8,128)(2,1)S(1)} %get-tuple-element.7.up_in, bf16[1024,2048]{1,0:T(8,128)(2,1)S(1)} %get-tuple-element.8.dn_in), custom_call_target="tpu_custom_call" | custom-call | tf_op jit(solution)/shard_map/pallas_call | solution.py:527

commit v4 on v3

--- a/solution.py
+++ b/solution.py
@@ -22,9 +22,8 @@
 
 def plan(Z, B, k, S, C):
     early = C // 2
-    steps = [("exchange",), ("share", 0), ("down",), ("down across", 0, C, True), ("down across", 0, early, False)]
-    steps += [("greet", i) for i in range(Z)]
-    steps += [("owned",)] + [("share", e) for e in range(1, B)]
+    steps = [("exchange",)] + [("share", e) for e in range(B)] + [("down",), ("down across", 0, C, True), ("down across", 0, early, False)]
+    steps += [("greet",), ("owned",)]
     steps += [("pass", j, s) for s in range(S) for j in range(k)]
     for far in range(Z - 1):
         steps += [("direct", far, s) for s in range(S)]
@@ -101,37 +100,26 @@
 
     barrier = pltpu.get_barrier_semaphore()
     below, above = z > 0, z < Z - 1
-    line = below.astype(jnp.int32) + above.astype(jnp.int32)
-
-    def greet(sem, wide):
-        def tell(dev):
-            pl.semaphore_signal(sem, inc=1, device_id=dev, device_id_type=MESH)
-
-        pl.when(above)(lambda: tell((g, f + Y, t)))
-        pl.when(below)(lambda: tell((g, f - Y, t)))
+
+    def tell(sem, dev):
+        pl.semaphore_signal(sem, inc=1, device_id=dev, device_id_type=MESH)
+
+    def tell_across(sem):
         for o in range(1, Y):
-            tell((g, z * Y + (y + o) % Y, t))
-        if wide:
-            for o in range(1, G):
-                tell(((g + o) % G, f, t))
-            for o in range(1, T):
-                tell((g, f, (t + o) % T))
+            tell(sem, (g, z * Y + (y + o) % Y, t))
+
+    def tell_chip(sem):
+        for o in range(1, T):
+            tell(sem, (g, f, (t + o) % T))
 
     for at in list(range(B, B + 1 + G)) + list(range(B)) + [B + 1 + G]:
         loads[at].start()
-    greet(barrier, True)
-
-    rounds = Z
-    greeted = [0]
-
-    def next_round():
-        if greeted[0] < rounds:
-            greet(hand.at[greeted[0]], False)
-            greeted[0] += 1
-
-    def round_over(i):
-        if i < rounds:
-            pl.semaphore_wait(hand.at[i], line + (Y - 1))
+    for o in range(1, Z):
+        tell(barrier, (g, ((z + o) % Z) * Y + y, t))
+    for o in range(1, G):
+        tell(barrier, ((g + o) % G, f, t))
+    tell_across(barrier)
+    tell_chip(barrier)
 
     loads[B].wait()
     wide_gain = jnp.broadcast_to(gain_v[...], (128, rows))
@@ -261,9 +249,11 @@
         on_tokens(zl * Y + y, e, lower, lower & above, None)
         on_tokens(zu * Y + y, e, upper, None, upper & below)
 
-    def greet_round(i):
-        round_over(i)
-        next_round()
+    def greet_rest():
+        pl.semaphore_wait(hand.at[0], (Y - 1) + (T - 1))
+        tell_chip(hand.at[1])
+        if T > 1:
+            pl.semaphore_wait(hand.at[1], T - 1)
 
     def on_pieces(far, s, relay):
         for c, cond in pieces_at(far):
@@ -273,12 +263,13 @@
         copy.wait()
     for h in range(G):
         convert_up(h)
-    pl.semaphore_wait(barrier, line + (Y - 1) + (G - 1) + (T - 1))
-    next_round()
+    pl.semaphore_wait(barrier, (Z - 1) + (G - 1) + (Y - 1) + (T - 1))
+    tell_across(hand.at[0])
+    tell_chip(hand.at[0])
     for step_name in plan(Z, B, k, S, C):
         kind, *at = step_name
         {
-            "share": share_tokens, "exchange": start_exchange, "greet": greet_round,
+            "share": share_tokens, "exchange": start_exchange, "greet": greet_rest,
             "owned": start_owned, "pass": from_exchange, "tokens": tokens_at, "down": start_down,
             "down across": down_across,
             "direct": lambda far, s: on_pieces(far, s, relay_direct), "far": lambda far, s: on_pieces(far, s, relay_far),
@@ -482,7 +473,7 @@
     unit = cols * G * T // n
     k = n // (G * T)
     E = 4 if here % 128 == 0 else 1
-    B = 2 if E % 2 == 0 else 1
+    B = E
     S, C, LAG, INNER = 1, 4, 2, 2
     width = rows * n
     feat = dcols * G * T // n
@@ -515,7 +506,7 @@
             pltpu.VMEM((Z, Y, here, feat), bf),
             pltpu.VMEM((Z, here, feat), bf),
             pltpu.VMEM((Z, here, feat), bf),
-            dma((G + 2,)), pltpu.SemaphoreType.REGULAR((Z,)), dma((sends,)),
+            dma((G + 2,)), pltpu.SemaphoreType.REGULAR((2,)), dma((sends,)),
             dma((n, B)), dma((k, G, S)), dma((n, G, S)), dma((G * T, C)),
             dma((Z, Y, E)), dma((Z, E)), dma((Z, E)), dma((G * T, T, C)), dma((Z, Y, E)), dma((Z, E)), dma((Z, E)),
         ],

time: 118 us -> 117 us (level)
  no operation moved by 1% of the time
where the time goes in v4:
time: 117 us
  Pallas kernels  116 us (99%)
    pallas_call x1, Pallas kernels, shards(): pl.pallas_call(functools.partial(kernel, G, n, T, Z, Y, k, E, B, S, C, LA...  112 us
    pallas_call x1, Pallas kernels, shards(): pl.pallas_call(functools.partial(drain, cuts), out_shape=tuple((jax.Shape...  3.52 us

profile of v4, /device:TPU:0, one launch (start us, length us, event | category | flops | bytes accessed | tf_op | source)
XLA Modules:
  0.0 116.6 jit_solution(5557834279608126426)
XLA Ops:
  0.6 112.5 %shard_map.67 = (bf16[256,1024]{1,0:T(8,128)(2,1)S(1)}, bf16[2048,1024]{1,0:T(8,128)(2,1)S(1)}, bf16[1024,2048]{1,0:T(8,128)(2,1)S(1)}) custom-call(bf16[1024,256]{1,0:T(8,128)(2,1)} %tok_ref.1, f32[1,256]{1,0:T(1,128)} %bitcast.1, f32[256,2048]{1,0:T(8,128)} %upw_ref.1, f32[1024,512]{1,0:T(8,128)} %dnw_ref.1), custom_call_target="tpu_custom_call" | custom-call | tf_op jit(solution)/shard_map/pallas_call | solution.py:487
  113.1 3.5 %shard_map.68 = (bf16[256,1024]{1,0:T(8,128)(2,1)}, bf16[2048,1024]{1,0:T(8,128)(2,1)}, bf16[1024,2048]{1,0:T(8,128)(2,1)}) custom-call(bf16[256,1024]{1,0:T(8,128)(2,1)S(1)} %get-tuple-element.6.mixed_in, bf16[2048,1024]{1,0:T(8,128)(2,1)S(1)} %get-tuple-element.7.up_in, bf16[1024,2048]{1,0:T(8,128)(2,1)S(1)} %get-tuple-element.8.dn_in), custom_call_target="tpu_custom_call" | custom-call | tf_op jit(solution)/shard_map/pallas_call | solution.py:518

commit v5 on v4

--- a/solution.py
+++ b/solution.py
@@ -29,8 +29,10 @@
         steps += [("direct", far, s) for s in range(S)]
         if far + 2 == Z:
             steps += [("direct", Z - 1, s) for s in range(S)] + [("down across", early, C, False)]
-        steps += [("tokens", far + 1, e) for e in range(B)]
-    steps += [("far", far, s) for s in range(S) for far in range(Z)]
+        for e in range(B):
+            steps += [("tokens", far + 1, e)]
+            if far + 2 == Z:
+                steps += [("far", at, s) for s in range(S) for at in range(e * Z // B, (e + 1) * Z // B)]
     return steps
 
 
@@ -336,7 +338,7 @@
         for o in range(1, Y):
             cross_copy(zd, o, e).start()
 
-    rstep = chunks(slab, 32)
+    rstep = chunks(slab, 64)
     fstep = chunks(slab, 128)
 
     def add_up(c, e, extras, final=False):

time: 117 us -> 117 us (level)
  no operation moved by 1% of the time
where the time goes in v5:
time: 117 us; the launch traced here: 116 us
  Pallas kernels  116 us (99%)
    pallas_call x1, Pallas kernels, shards(): pl.pallas_call(functools.partial(kernel, G, n, T, Z, Y, k, E, B, S, C, LA...  112 us
    pallas_call x1, Pallas kernels, shards(): pl.pallas_call(functools.partial(drain, cuts), out_shape=tuple((jax.Shape...  3.52 us

profile of v5, /device:TPU:0, one launch (start us, length us, event | category | flops | bytes accessed | tf_op | source)
XLA Modules:
  0.0 116.4 jit_solution(16027608547372989911)
XLA Ops:
  0.6 112.2 %shard_map.67 = (bf16[256,1024]{1,0:T(8,128)(2,1)S(1)}, bf16[2048,1024]{1,0:T(8,128)(2,1)S(1)}, bf16[1024,2048]{1,0:T(8,128)(2,1)S(1)}) custom-call(bf16[1024,256]{1,0:T(8,128)(2,1)} %tok_ref.1, f32[1,256]{1,0:T(1,128)} %bitcast.1, f32[256,2048]{1,0:T(8,128)} %upw_ref.1, f32[1024,512]{1,0:T(8,128)} %dnw_ref.1), custom_call_target="tpu_custom_call" | custom-call | tf_op jit(solution)/shard_map/pallas_call | solution.py:489
  112.8 3.5 %shard_map.68 = (bf16[256,1024]{1,0:T(8,128)(2,1)}, bf16[2048,1024]{1,0:T(8,128)(2,1)}, bf16[1024,2048]{1,0:T(8,128)(2,1)}) custom-call(bf16[256,1024]{1,0:T(8,128)(2,1)S(1)} %get-tuple-element.6.mixed_in, bf16[2048,1024]{1,0:T(8,128)(2,1)S(1)} %get-tuple-element.7.up_in, bf16[1024,2048]{1,0:T(8,128)(2,1)S(1)} %get-tuple-element.8.dn_in), custom_call_target="tpu_custom_call" | custom-call | tf_op jit(solution)/shard_map/pallas_call | solution.py:520
